TPU v7x, 32 devices: a whole 2x2x4 slice. The times are simulated.
32 devices in a mesh: rep: 2 (over x), fs: 8 (over z, y), tp: 2 (over core).
Axes of the slice: x: 2, y: 2, z: 4, core: 2. Of those that a mesh axis runs over, the one named last changes fastest.
Arguments:
- activations: bfloat16 [16384, 1024], P(('rep', 'fs', 'tp')), may hold values from -8 to 8
- mixer_gain: float32 [1024], replicated, may hold values from 0.1 to 1.9
- query_weight: bfloat16 [1024, 256], P('fs', 'tp'), may hold values from -0.1875 to 0.1875
- key_weight: bfloat16 [1024, 256], P('fs', 'tp'), may hold values from -0.1875 to 0.1875
- value_weight: bfloat16 [1024, 512], P('fs', 'tp'), may hold values from -0.1875 to 0.1875
- rank_weight: bfloat16 [1024, 16], replicated, may hold values from -0.1875 to 0.1875
- decay_gate_weight: bfloat16 [16, 256], P(None, 'tp'), may hold values from -1.5 to 1.5
- decay_gate_bias: float32 [256], P('tp'), may hold values from -1.5 to 8
- head_gain: float32 [256], replicated, may hold values from 0.1 to 1.9
- output_weight: bfloat16 [512, 1024], P('tp', 'fs'), may hold values from -0.25 to 0.25
- ffn_gain: float32 [1024], replicated, may hold values from 0.1 to 1.9
- gate_weight: bfloat16 [1024, 2816], P('fs', 'tp'), may hold values from -0.1875 to 0.1875
- up_weight: bfloat16 [1024, 2816], P('fs', 'tp'), may hold values from -0.1875 to 0.1875
- down_weight: bfloat16 [2816, 1024], P('tp', 'fs'), may hold values from -0.109375 to 0.109375
Outputs:
- result: bfloat16 [16384, 1024], P(('rep', 'fs', 'tp'))
All inputs are finite; a program needn't handle non-finite values.
Results may differ from a plain program's by a relative error of at most 0.0056.
Values may be sent and summed in bfloat16 or wider, within the bound.
No kernel may reach another device: no remote copies, remote signals or barrier semaphores. Data moves between devices by JAX's collectives and lax.ppermute only.
A program may use at most 64 MiB of HBM per device.

v0:
```python
import jax
import jax.numpy as jnp
from jax import lax
from jax.sharding import PartitionSpec as P

DK = 128
DV = 256
BLOCK = 64
epsilon = 1e-06
decay_softness = 16.0
highest = lax.Precision.HIGHEST


def rms_scale(values, gains):
    return values * lax.rsqrt(jnp.mean(values * values, axis=-1, keepdims=True) + epsilon) * gains


def linear_attention(queries, keys_all, values_all, decay_logarithm, head_count):
    length = queries.shape[0]
    number = length // BLOCK
    halfway = BLOCK // 2
    causal = jnp.tril(jnp.ones((BLOCK, BLOCK), bool))

    def to_blocks(matrix):
        return matrix.astype(jnp.float32).reshape(
            number, BLOCK, head_count, matrix.shape[1] // head_count
        )

    block_query = to_blocks(queries)
    block_key = to_blocks(keys_all)
    block_value = to_blocks(values_all)
    cumulative = jnp.cumsum(to_blocks(decay_logarithm), axis=1)
    middle = cumulative[:, halfway - 1 : halfway]
    query_local = block_query * jnp.exp(cumulative - middle)
    key_local = block_key * jnp.exp(middle - cumulative)
    scores = jnp.einsum("nthd,nshd->nhts", query_local, key_local, precision=highest)
    scores = jnp.where(causal[None, None], scores, 0.0)
    within = jnp.einsum("nhts,nshv->nthv", scores, block_value, precision=highest)
    lasting = cumulative[:, -1]
    update = jnp.einsum(
        "nshd,nshv->nhdv",
        block_key * jnp.exp(lasting[:, None] - cumulative),
        block_value,
        precision=highest,
    )

    def advance(memory, inputs):
        fade, addition = inputs
        return (jnp.exp(fade)[:, :, None] * memory + addition, memory)

    key_width = queries.shape[1] // head_count
    value_width = values_all.shape[1] // head_count
    initial = jnp.zeros((head_count, key_width, value_width), jnp.float32)
    earlier = lax.scan(advance, initial, (lasting, update))[1]
    carried = jnp.einsum(
        "nthd,nhdv->nthv", block_query * jnp.exp(cumulative), earlier, precision=highest
    )
    return (within + carried).reshape(length, head_count, value_width)


def project_inputs(source, weight):
    return jnp.dot(source, weight, preferred_element_type=jnp.float32)


def local(
    activations,
    mixer_gain,
    query_weight,
    key_weight,
    value_weight,
    rank_weight,
    decay_gate_weight,
    decay_gate_bias,
    head_gain,
    output_weight,
    ffn_gain,
    gate_weight,
    up_weight,
    down_weight,
):
    residual = activations.astype(jnp.float32)
    normed = rms_scale(residual, mixer_gain).astype(jnp.bfloat16)
    rank_slice = project_inputs(normed, rank_weight).astype(jnp.bfloat16)
    sequence, rank_slices_gathered = (
        lax.all_gather(normed, "tp", axis=0, tiled=True),
        lax.all_gather(rank_slice, "tp", axis=0, tiled=True),
    )
    length = sequence.shape[0]
    query_full, key_full, value_full = (
        lax.all_gather(query_weight, "fs", axis=0, tiled=True),
        lax.all_gather(key_weight, "fs", axis=0, tiled=True),
        lax.all_gather(value_weight, "fs", axis=0, tiled=True),
    )
    queries = project_inputs(sequence, query_full).astype(jnp.bfloat16)
    keys_all = project_inputs(sequence, key_full).astype(jnp.bfloat16)
    values_all = project_inputs(sequence, value_full).astype(jnp.bfloat16)
    decay_logarithm = (
        jax.nn.log_sigmoid(
            project_inputs(rank_slices_gathered, decay_gate_weight) + decay_gate_bias
        )
        / decay_softness
    )
    head_count = query_weight.shape[1] // DK
    attended = linear_attention(queries, keys_all, values_all, decay_logarithm, head_count)
    head_rows = rms_scale(attended, head_gain).astype(jnp.bfloat16).reshape(length, head_count * DV)
    own_rows = lax.all_to_all(head_rows, "tp", split_axis=0, concat_axis=1, tiled=True)
    tall_out = lax.all_gather(output_weight, "tp", axis=0, tiled=True)
    whole_out = lax.all_gather(tall_out, "fs", axis=1, tiled=True)
    mixed = residual + project_inputs(own_rows, whole_out)
    ffn_normed = rms_scale(mixed, ffn_gain).astype(jnp.bfloat16)
    ffn_sequence = lax.all_gather(ffn_normed, "tp", axis=0, tiled=True)
    gate_full, up_full = (
        lax.all_gather(gate_weight, "fs", axis=0, tiled=True),
        lax.all_gather(up_weight, "fs", axis=0, tiled=True),
    )
    down_full = lax.all_gather(down_weight, "fs", axis=1, tiled=True)
    hidden = (
        jax.nn.silu(project_inputs(ffn_sequence, gate_full)) * project_inputs(ffn_sequence, up_full)
    ).astype(jnp.bfloat16)
    result = mixed + lax.psum_scatter(
        project_inputs(hidden, down_full).astype(jnp.bfloat16),
        "tp",
        scatter_dimension=0,
        tiled=True,
    ).astype(jnp.float32)
    return result.astype(jnp.bfloat16)


def solution(mesh):
    in_specs = (
        P(("rep", "fs", "tp"), None),
        P(),
        P("fs", "tp"),
        P("fs", "tp"),
        P("fs", "tp"),
        P(),
        P(None, "tp"),
        P("tp"),
        P(),
        P("tp", "fs"),
        P(),
        P("fs", "tp"),
        P("fs", "tp"),
        P("tp", "fs"),
    )
    out_specs = P(("rep", "fs", "tp"), None)
    return jax.shard_map(local, mesh=mesh, in_specs=in_specs, out_specs=out_specs, check_vma=False)
```

profile of v0, /device:TPU:0, one launch (start us, length us, event | category | flops | bytes accessed | tf_op | source)
XLA Modules:
  0.0 369.9 jit_solution(17549334003282702146)
XLA Ops:
  6.5 1.5 fusion.2
  8.1 2.5 fusion.4
  10.7 2.2 all_gather.38
  13.0 1.6 convolution_convert_fusion.3
  14.6 2.1 all_gather.36
  16.8 0.5 fusion.12
  17.2 0.3 fusion.24
  17.6 32.6 %all_gather.37 = bf16[1024,128]{1,0:T(8,128)(2,1)S(1)} all-gather(bf16[128,128]{1,0:T(8,128)(2,1)S(1)} %copy-done.8), channel_id=1, replica_groups=mesh['rep'=2,'fs'=8,'tp'=2] {'fs'}, dimensions={0}, use_global_device_ids=true | all-gather | bytes 294912 | tf_op jit(solution)/shard_map/all_gather | solution.py:91
  50.2 31.1 %all_gather.35 = bf16[1024,128]{1,0:T(8,128)(2,1)S(1)} all-gather(bf16[128,128]{1,0:T(8,128)(2,1)S(1)} %copy-done.9), channel_id=1, replica_groups=mesh['rep'=2,'fs'=8,'tp'=2] {'fs'}, dimensions={0}, use_global_device_ids=true | all-gather | bytes 294912 | tf_op jit(solution)/shard_map/all_gather | solution.py:90
  81.3 31.3 %all_gather.34 = bf16[1024,256]{1,0:T(8,128)(2,1)S(1)} all-gather(bf16[128,256]{1,0:T(8,128)(2,1)S(1)} %copy-done.7), channel_id=1, replica_groups=mesh['rep'=2,'fs'=8,'tp'=2] {'fs'}, dimensions={0}, use_global_device_ids=true | all-gather | bytes 589824 | tf_op jit(solution)/shard_map/all_gather | solution.py:92
  112.6 2.4 convolution_convert_fusion.1
  115.1 0.7 convolution_convert_fusion.2
  115.8 1.6 fusion.14
  117.4 0.7 convolution_convert_fusion
  118.1 1.1 convolution_bitcast_fusion
  119.2 12.6 %while.13 = (s32[]{:T(128)}, f32[1,128,256]{2,1,0:T(8,128)S(1)}, f32[16,1,128,256]{3,2,1,0:T(8,128)}, f32[16,1,128]{2,1,0:T(1,128)S(1)}, f32[16,1,128,256]{3,2,1,0:T(8,128)S(1)}, /*index=5*/s32[]{:T(128)}, s32[]{:T(128)}) while((s32[]{:T(128)}, f32[1,128,256]{2,1,0:T(8,128)S(1)}, f32[16,1,128,256]{3,2,1,0:T(8,128)}, ...), condition=%wide.region_3.4_spmd.clone, body=%wide.region_2.3_spmd.clone.sunk | while | flops 131075 | bytes 657504 | solution.py:54
  119.2 0.7 bitcast_dynamic-update-slice_fusion.2
  119.9 0.1 bitcast_add_fusion.2
  120.0 0.7 bitcast_dynamic-update-slice_fusion.2
  120.7 0.1 bitcast_add_fusion.2
  120.8 0.7 bitcast_dynamic-update-slice_fusion.2
  121.4 0.1 bitcast_add_fusion.2
  121.6 0.7 bitcast_dynamic-update-slice_fusion.2
  122.2 0.1 bitcast_add_fusion.2
  122.3 0.7 bitcast_dynamic-update-slice_fusion.2
  123.0 0.1 bitcast_add_fusion.2
  123.1 0.7 bitcast_dynamic-update-slice_fusion.2
  123.8 0.1 bitcast_add_fusion.2
  123.9 0.6 bitcast_dynamic-update-slice_fusion.2
  124.6 0.1 bitcast_add_fusion.2
  124.7 0.7 bitcast_dynamic-update-slice_fusion.2
  125.4 0.1 bitcast_add_fusion.2
  125.5 0.7 bitcast_dynamic-update-slice_fusion.2
  126.2 0.1 bitcast_add_fusion.2
  126.3 0.7 bitcast_dynamic-update-slice_fusion.2
  127.1 0.7 bitcast_dynamic-update-slice_fusion.2
  127.7 0.1 bitcast_add_fusion.2
  127.9 0.7 bitcast_dynamic-update-slice_fusion.2
  128.7 0.7 bitcast_dynamic-update-slice_fusion.2
  129.4 0.7 bitcast_dynamic-update-slice_fusion.2
  130.2 0.7 bitcast_dynamic-update-slice_fusion.2
  131.0 0.7 bitcast_dynamic-update-slice_fusion.2
  131.8 2.2 convolution_select_fusion
  134.1 3.0 fusion.5
  137.1 0.7 fusion.10
  137.8 0.3 copy.33
  138.3 0.9 multiply_convert_fusion.2
  139.2 3.5 all-to-all-start
  142.8 1.7 all-to-all-done
  144.4 0.8 copy-done.3
  145.2 2.2 multiply_reduce_fusion
  147.5 1.2 multiply_convert_fusion.1
  148.7 0.5 all-gather.13.cloned.1.call-update
  149.3 0.5 all-gather.15.cloned.1.call-update
  149.9 0.5 all-gather.17.cloned.1.call-update
  150.4 0.2 reduce-scatter.2.cloned.1.call-start
  150.7 10.0 %all-gather.11.cloned.1.call-done = bf16[1024,1024]{1,0:T(8,128)(2,1)} async-done(((bf16[512,1024]{1,0:T(8,128)(2,1)}), bf16[1024,1024]{1,0:T(8,128)(2,1)}) %all-gather.11.cloned.1.call-update) | async-done | bytes 2097168 | tf_op jit(solution)/shard_map/all_gather | solution.py:111
  160.7 60.5 %all-gather.13.cloned.1.call-done = bf16[1024,1408]{1,0:T(8,128)(2,1)} async-done(((bf16[128,1408]{1,0:T(8,128)(2,1)}), bf16[1024,1408]{1,0:T(8,128)(2,1)}) %all-gather.13.cloned.1.call-update) | async-done | bytes 2883600 | tf_op jit(solution)/shard_map/all_gather | solution.py:113
  221.2 8.3 %fusion.27 = f32[1024,1408]{1,0:T(8,128)} fusion(bf16[1024,1024]{1,0:T(8,128)(2,1)} %all-gather.11.cloned.1.call-done, bf16[1024,1408]{1,0:T(8,128)(2,1)} %all-gather.13.cloned.1.call-done), kind=kOutput, calls=%fused_computation.58 | convolution fusion | flops 2952790016 | bytes 10747904 | tf_op jit(solution)/shard_map/dot_general | solution.py:62
  229.6 49.6 %all-gather.15.cloned.1.call-done = bf16[1024,1408]{1,0:T(8,128)(2,1)} async-done(((bf16[128,1408]{1,0:T(8,128)(2,1)}), bf16[1024,1408]{1,0:T(8,128)(2,1)}) %all-gather.15.cloned.1.call-update) | async-done | bytes 2883600 | tf_op jit(solution)/shard_map/all_gather | solution.py:114
  279.2 60.1 %all-gather.17.cloned.1.call-done = bf16[1408,1024]{1,0:T(8,128)(2,1)} async-done(((bf16[1408,128]{1,0:T(8,128)(2,1)}), bf16[1408,1024]{1,0:T(8,128)(2,1)}) %all-gather.17.cloned.1.call-update) | async-done | bytes 2883600 | tf_op jit(solution)/shard_map/all_gather | solution.py:116
  339.3 13.1 %fusion.8 = bf16[1024,1024]{1,0:T(8,128)(2,1)} fusion(bf16[1408,1024]{1,0:T(8,128)(2,1)} %all-gather.17.cloned.1.call-done, f32[1024,1408]{1,0:T(8,128)} %fusion.27, bf16[1024,1024]{1,0:T(8,128)(2,1)} %all-gather.11.cloned.1.call-done, bf16[1024,1408]{1,0:T(8,128)(2,1)} %all-gather.15.cloned.1.call-done), kind=kOutput, calls=%fused_computation.18 | convolution fusion | flops 5915279360 | bytes 15728640 | tf_op jit(solution)/shard_map/dot_general | solution.py:62
  352.4 8.1 %reduce-scatter.2.cloned.1.call-done = bf16[512,1024]{1,0:T(8,128)(2,1)} async-done(((bf16[1024,1024]{1,0:T(8,128)(2,1)}), bf16[512,1024]{1,0:T(8,128)(2,1)}) %reduce-scatter.2.cloned.1.call-update) | async-done | bytes 1048592 | tf_op jit(solution)/shard_map/reduce_scatter | solution.py:120
  360.5 2.5 add_convert_fusion
  (71 shorter events, 1.2 us)
Async XLA Ops:
  6.5 6.4 %copy-start = (bf16[1024,16]{0,1:T(8,128)(2,1)S(1)}, bf16[1024,16]{0,1:T(8,128)(2,1)}, u32[]{:S(2)}) copy-start(bf16[1024,16]{0,1:T(8,128)(2,1)} %param.21) | copy-start | bytes 98308
  6.5 106.0 %all-gather.7.cloned.1.call-start = ((), (), s32[]{:S(2)}) async-start(), calls=%async_computation.2 | async-start | bytes 3145728 | tf_op jit(solution)/shard_map/all_gather | solution.py:85
  6.5 4.2 %copy-start.6 = (bf16[256,128]{1,0:T(8,128)(2,1)S(1)}, bf16[256,128]{1,0:T(8,128)(2,1)}, u32[]{:S(2)}) copy-start(bf16[256,128]{1,0:T(8,128)(2,1)} %param.25) | copy-start | bytes 196612
  8.1 8.7 %copy-start.12 = (bf16[16,128]{1,0:T(8,128)(2,1)S(1)}, bf16[16,128]{1,0:T(8,128)(2,1)}, u32[]{:S(2)}) copy-start(bf16[16,128]{1,0:T(8,128)(2,1)} %param.22) | copy-start | bytes 12292
  8.1 8.7 %copy-start.13 = (f32[128]{0:T(128)S(1)}, f32[128]{0:T(128)}, u32[]{:S(2)}) copy-start(f32[128]{0:T(128)} %param.23) | copy-start | bytes 1540
  10.7 132.1 %all-gather.9.cloned.1.call-start = ((), (), s32[]{:S(2)}) async-start(), calls=%async_computation.3 | async-start | bytes 1179648 | tf_op jit(solution)/shard_map/all_gather | solution.py:108
  13.0 4.6 %copy-start.8 = (bf16[128,128]{1,0:T(8,128)(2,1)S(1)}, bf16[128,128]{1,0:T(8,128)(2,1)}, u32[]{:S(2)}) copy-start(bf16[128,128]{1,0:T(8,128)(2,1)} %param.19) | copy-start | bytes 98308
  14.6 35.6 %copy-start.9 = (bf16[128,128]{1,0:T(8,128)(2,1)S(1)}, bf16[128,128]{1,0:T(8,128)(2,1)}, u32[]{:S(2)}) copy-start(bf16[128,128]{1,0:T(8,128)(2,1)} %param.18) | copy-start | bytes 98308
  14.6 66.6 %copy-start.7 = (bf16[128,256]{1,0:T(8,128)(2,1)S(1)}, bf16[128,256]{1,0:T(8,128)(2,1)}, u32[]{:S(2)}) copy-start(bf16[128,256]{1,0:T(8,128)(2,1)} %param.20) | copy-start | bytes 196612
  112.6 2.5 copy-start.2
  118.1 1.1 copy-start.4
  134.0 3.0 copy-start.5
  137.1 1.2 copy-start.11
  137.8 7.4 %copy-start.1 = (bf16[512,1024]{1,0:T(8,128)(2,1)S(1)}, bf16[512,1024]{1,0:T(8,128)(2,1)}, u32[]{:S(2)}) copy-start(bf16[512,1024]{1,0:T(8,128)(2,1)} %param.16) | copy-start | bytes 3145732
  139.2 5.2 %all-to-all-start = ((bf16[2,512,256]{1,2,0:T(8,128)(2,1)}), bf16[2,512,256]{1,2,0:T(8,128)(2,1)S(1)}, u32[]{:S(2)}, u32[]{:S(2)}) async-start(bf16[2,512,256]{1,2,0:T(8,128)(2,1)} %multiply_convert_fusion.2), calls=%async_computation | async-start | bytes 1048576 | tf_op jit(solution)/shard_map/all_to_all | solution.py:106
  142.7 18.0 %all-gather.11.cloned.1.call-start = ((), (), s32[]{:S(2)}) async-start(), calls=%async_computation.4 | async-start | bytes 3145728 | tf_op jit(solution)/shard_map/all_gather | solution.py:111
  144.4 0.8 copy-start.3
  145.2 2.2 copy-start.10
  148.7 72.5 %all-gather.13.cloned.1.call-start = ((), (), s32[]{:S(2)}) async-start(), calls=%async_computation.5 | async-start | bytes 3244032 | tf_op jit(solution)/shard_map/all_gather | solution.py:113
  149.3 129.9 %all-gather.15.cloned.1.call-start = ((), (), s32[]{:S(2)}) async-start(), calls=%async_computation.6 | async-start | bytes 3244032 | tf_op jit(solution)/shard_map/all_gather | solution.py:114
  149.9 189.5 %all-gather.17.cloned.1.call-start = ((), (), s32[]{:S(2)}) async-start(), calls=%async_computation.7 | async-start | bytes 3244032 | tf_op jit(solution)/shard_map/all_gather | solution.py:116
  150.4 210.1 %reduce-scatter.2.cloned.1.call-start = ((), (), s32[]{:S(2)}) async-start(), calls=%async_computation.8 | async-start | bytes 3145728 | tf_op jit(solution)/shard_map/reduce_scatter | solution.py:120
Sparse Core Ops, SparseCore 0:
  10.8 13.2 all-gather.6
  26.1 42.2 all-gather.8
  148.8 11.8 all-gather.10
  162.7 58.4 all-gather.12
  223.3 55.9 all-gather.14
  281.1 58.1 all-gather.16
  352.5 7.9 reduce-scatter.1
where the time goes:
time: 370 us
  waiting for transfers between devices  192 us (52%)
  blocking collectives  99.3 us (27%)
  matrix products  36.6 us (10%)
  other arithmetic  22.9 us (6%)
  between operations  13.8 us (4%)
  starting transfers between devices  3.91 us (1%)
    all_gather x1, waiting for transfers between devices, local(): lax.all_gather(gate_weight, 'fs', axis=0, tiled=True)  60.5 us
    all_gather x1, waiting for transfers between devices, local(): down_full = lax.all_gather(down_weight, 'fs', axis=1, tiled=True)  60.1 us
    all_gather x1, waiting for transfers between devices, local(): lax.all_gather(up_weight, 'fs', axis=0, tiled=True)  49.6 us
    all_gather x1, blocking collectives, local(): lax.all_gather(key_weight, 'fs', axis=0, tiled=True)  32.6 us
    all_gather x1, blocking collectives, local(): lax.all_gather(value_weight, 'fs', axis=0, tiled=True)  31.3 us
    all_gather x1, blocking collectives, local(): lax.all_gather(query_weight, 'fs', axis=0, tiled=True)  31.1 us
    dot_general x8, matrix products, project_inputs(): return jnp.dot(source, weight, preferred_element_type=jnp.float32)  29.6 us
    dynamic_update_slice x16, other arithmetic, linear_attention(): earlier = lax.scan(advance, initial, (lasting, update))[1]  10.6 us
  transfers between devices with their start and end apart: 8, of which 6 were waited for; matrix products, arithmetic and copies ran while one was open for 10% of the time, Pallas kernels for 0%

commit v1 on v0

--- a/solution.py
+++ b/solution.py
@@ -113,7 +113,13 @@
         lax.all_gather(gate_weight, "fs", axis=0, tiled=True),
         lax.all_gather(up_weight, "fs", axis=0, tiled=True),
     )
-    down_full = lax.all_gather(down_weight, "fs", axis=1, tiled=True)
+    size = lax.axis_size("fs")
+    held, tiles = (down_weight, [down_weight])
+    for _ in range(size - 1):
+        held = lax.ppermute(held, "fs", [(i, (i + 1) % size) for i in range(size)])
+        tiles.insert(0, held)
+    row_of_blocks = jnp.concatenate(tiles, axis=1)
+    down_full = jnp.roll(row_of_blocks, (lax.axis_index("fs") + 1) * down_weight.shape[1], axis=1)
     hidden = (
         jax.nn.silu(project_inputs(ffn_sequence, gate_full)) * project_inputs(ffn_sequence, up_full)
     ).astype(jnp.bfloat16)

time: 370 us -> 335 us (0.905)
  waiting for transfers between devices: 192 us -> 133 us
  local copies, waits for them, and re-layouts: 1.33 us -> 22.7 us
    ppermute x0 -> x7, waiting for transfers between devices: none -> 104 us  [local(): held = lax.ppermute(held, 'fs', [(i, (i + 1) % size) for i in range(size)])]
    all_gather x1, waiting for transfers between devices: 60.5 us -> 0.01 us  [local(): lax.all_gather(gate_weight, 'fs', axis=0, tiled=True)]
    all_gather x1 -> x0, waiting for transfers between devices: 60.1 us -> none  [local(): down_full = lax.all_gather(down_weight, 'fs', axis=1, tiled=True)]
    all_gather x1, waiting for transfers between devices: 49.6 us -> 18.4 us  [local(): lax.all_gather(up_weight, 'fs', axis=0, tiled=True)]
    unnamed x28 -> x53, local copies, waits for them, and re-layouts: 0.86 us -> 21.5 us
    all_gather x1, waiting for transfers between devices: 10 us -> 0.01 us  [local(): ffn_sequence = lax.all_gather(ffn_normed, 'tp', axis=0, tiled=True)]
  transfers between devices with their start and end apart: 8 -> 14, of which waited for: 6 -> 10; matrix products, arithmetic and copies ran while one was open for 10% -> 17% of each run, Pallas kernels for 0% -> 0%
where the time goes in v1:
time: 335 us; the launch traced here: 334 us
  waiting for transfers between devices  133 us (40%)
  blocking collectives  99.6 us (30%)
  matrix products  36.6 us (11%)
  other arithmetic  22.9 us (7%)
  local copies, waits for them, and re-layouts  22.7 us (7%)
  between operations  13.8 us (4%)
  starting transfers between devices  5.41 us (2%)
    ppermute x7, waiting for transfers between devices, local(): held = lax.ppermute(held, 'fs', [(i, (i + 1) % size) for i in range(size)])  104 us
    all_gather x1, blocking collectives, local(): lax.all_gather(value_weight, 'fs', axis=0, tiled=True)  33.3 us
    all_gather x1, blocking collectives, local(): lax.all_gather(query_weight, 'fs', axis=0, tiled=True)  31.4 us
    all_gather x1, blocking collectives, local(): lax.all_gather(key_weight, 'fs', axis=0, tiled=True)  30.7 us
    dot_general x8, matrix products, project_inputs(): return jnp.dot(source, weight, preferred_element_type=jnp.float32)  29.5 us
    unnamed x53, local copies, waits for them, and re-layouts  21.5 us
    all_gather x1, waiting for transfers between devices, local(): lax.all_gather(up_weight, 'fs', axis=0, tiled=True)  18.4 us
    dynamic_update_slice x16, other arithmetic, linear_attention(): earlier = lax.scan(advance, initial, (lasting, update))[1]  10.6 us
  transfers between devices with their start and end apart: 14, of which 10 were waited for; matrix products, arithmetic and copies ran while one was open for 17% of the time, Pallas kernels for 0%

profile of v1, /device:TPU:0, one launch (start us, length us, event | category | flops | bytes accessed | tf_op | source)
XLA Modules:
  0.0 334.3 jit_solution(17661143344697548970)
XLA Ops:
  6.6 1.5 fusion.4
  8.1 2.5 fusion.6
  10.7 2.2 all_gather.35
  13.0 1.6 convolution_convert_fusion.3
  14.6 2.0 all_gather.33
  17.4 33.3 %all_gather.31 = bf16[1024,256]{1,0:T(8,128)(2,1)S(1)} all-gather(bf16[128,256]{1,0:T(8,128)(2,1)S(1)} %copy-done.12), channel_id=1, replica_groups=mesh['rep'=2,'fs'=8,'tp'=2] {'fs'}, dimensions={0}, use_global_device_ids=true | all-gather | bytes 589824 | tf_op jit(solution)/shard_map/all_gather | solution.py:92
  50.7 31.4 %all_gather.32 = bf16[1024,128]{1,0:T(8,128)(2,1)S(1)} all-gather(bf16[128,128]{1,0:T(8,128)(2,1)S(1)} %copy-done.13), channel_id=1, replica_groups=mesh['rep'=2,'fs'=8,'tp'=2] {'fs'}, dimensions={0}, use_global_device_ids=true | all-gather | bytes 294912 | tf_op jit(solution)/shard_map/all_gather | solution.py:90
  82.1 30.7 %all_gather.34 = bf16[1024,128]{1,0:T(8,128)(2,1)S(1)} all-gather(bf16[128,128]{1,0:T(8,128)(2,1)S(1)} %copy-done.14), channel_id=1, replica_groups=mesh['rep'=2,'fs'=8,'tp'=2] {'fs'}, dimensions={0}, use_global_device_ids=true | all-gather | bytes 294912 | tf_op jit(solution)/shard_map/all_gather | solution.py:91
  112.8 2.4 convolution_convert_fusion.2
  115.3 0.7 convolution_convert_fusion.1
  116.1 1.6 fusion.17
  117.7 0.7 convolution_convert_fusion
  118.4 1.1 convolution_bitcast_fusion
  119.5 12.7 %while.13 = (s32[]{:T(128)}, f32[1,128,256]{2,1,0:T(8,128)S(1)}, f32[16,1,128,256]{3,2,1,0:T(8,128)}, f32[16,1,128]{2,1,0:T(1,128)S(1)}, f32[16,1,128,256]{3,2,1,0:T(8,128)S(1)}, /*index=5*/s32[]{:T(128)}, s32[]{:T(128)}) while((s32[]{:T(128)}, f32[1,128,256]{2,1,0:T(8,128)S(1)}, f32[16,1,128,256]{3,2,1,0:T(8,128)}, ...), condition=%wide.region_3.4_spmd.clone, body=%wide.region_2.3_spmd.clone.sunk | while | flops 131075 | bytes 657004 | solution.py:54
  119.5 0.7 bitcast_dynamic-update-slice_fusion.2
  120.3 0.7 bitcast_dynamic-update-slice_fusion.2
  121.1 0.7 bitcast_dynamic-update-slice_fusion.2
  121.9 0.7 bitcast_dynamic-update-slice_fusion.2
  124.2 0.7 bitcast_dynamic-update-slice_fusion.2
  125.8 0.7 bitcast_dynamic-update-slice_fusion.2
  127.4 0.7 bitcast_dynamic-update-slice_fusion.2
  128.2 0.7 bitcast_dynamic-update-slice_fusion.2
  129.0 0.7 bitcast_dynamic-update-slice_fusion.2
  131.4 0.7 bitcast_dynamic-update-slice_fusion.2
  132.1 2.3 convolution_select_fusion
  134.4 3.0 fusion.7
  137.4 0.7 fusion.13
  138.6 0.9 multiply_convert_fusion.2
  139.5 3.6 %all-to-all-start = ((bf16[2,512,256]{1,2,0:T(8,128)(2,1)}), bf16[2,512,256]{1,2,0:T(8,128)(2,1)S(1)}, u32[]{:S(2)}, u32[]{:S(2)}) async-start(bf16[2,512,256]{1,2,0:T(8,128)(2,1)} %multiply_convert_fusion.2), calls=%async_computation | async-start | bytes 1048576 | tf_op jit(solution)/shard_map/all_to_all | solution.py:106
  143.2 1.7 all-to-all-done
  144.9 0.8 copy-done.3
  145.7 2.2 multiply_reduce_fusion
  147.9 1.2 multiply_convert_fusion.1
  149.8 1.6 collective-permute-start
  151.4 11.6 %collective-permute-done = bf16[1408,128]{1,0:T(8,128)(2,1)S(1)} collective-permute-done((bf16[1408,128]{1,0:T(8,128)(2,1)S(1)}, bf16[1408,128]{1,0:T(8,128)(2,1)S(1)}, u32[]{:S(2)}, u32[]{:S(2)}) %collective-permute-start) | collective-permute-done | bytes 360480 | tf_op jit(solution)/shard_map/ppermute | solution.py:119
  163.0 12.3 %collective-permute-done.1 = bf16[1408,128]{1,0:T(8,128)(2,1)S(1)} collective-permute-done((bf16[1408,128]{1,0:T(8,128)(2,1)S(1)}, bf16[1408,128]{1,0:T(8,128)(2,1)S(1)}, u32[]{:S(2)}, u32[]{:S(2)}) %collective-permute-start.1) | collective-permute-done | bytes 360480 | tf_op jit(solution)/shard_map/ppermute | solution.py:119
  175.4 20.8 %collective-permute-done.2 = bf16[1408,128]{1,0:T(8,128)(2,1)S(1)} collective-permute-done((bf16[1408,128]{1,0:T(8,128)(2,1)S(1)}, bf16[1408,128]{1,0:T(8,128)(2,1)S(1)}, u32[]{:S(2)}, u32[]{:S(2)}) %collective-permute-start.2) | collective-permute-done | bytes 360480 | tf_op jit(solution)/shard_map/ppermute | solution.py:119
  196.2 0.8 copy-done.7
  196.9 16.4 %collective-permute-done.3 = bf16[1408,128]{1,0:T(8,128)(2,1)S(1)} collective-permute-done((bf16[1408,128]{1,0:T(8,128)(2,1)S(1)}, bf16[1408,128]{1,0:T(8,128)(2,1)S(1)}, u32[]{:S(2)}, u32[]{:S(2)}) %collective-permute-start.3) | collective-permute-done | bytes 360480 | tf_op jit(solution)/shard_map/ppermute | solution.py:119
  213.3 0.7 copy-done.9
  214.1 19.5 %collective-permute-done.4 = bf16[1408,128]{1,0:T(8,128)(2,1)} collective-permute-done((bf16[1408,128]{1,0:T(8,128)(2,1)S(1)}, bf16[1408,128]{1,0:T(8,128)(2,1)}, u32[]{:S(2)}, u32[]{:S(2)}) %collective-permute-start.4) | collective-permute-done | bytes 360480 | tf_op jit(solution)/shard_map/ppermute | solution.py:119
  233.7 12.5 %collective-permute-done.5 = bf16[1408,128]{1,0:T(8,128)(2,1)} collective-permute-done((bf16[1408,128]{1,0:T(8,128)(2,1)}, bf16[1408,128]{1,0:T(8,128)(2,1)}, u32[]{:S(2)}, u32[]{:S(2)}) %collective-permute-start.5) | collective-permute-done | bytes 360480 | tf_op jit(solution)/shard_map/ppermute | solution.py:119
  246.2 10.4 %collective-permute-done.6 = bf16[1408,128]{1,0:T(8,128)(2,1)} collective-permute-done((bf16[1408,128]{1,0:T(8,128)(2,1)}, bf16[1408,128]{1,0:T(8,128)(2,1)}, u32[]{:S(2)}, u32[]{:S(2)}) %collective-permute-start.6) | collective-permute-done | bytes 360480 | tf_op jit(solution)/shard_map/ppermute | solution.py:119
  256.7 1.8 constant_dynamic-update-slice_fusion.15
  258.4 1.8 constant_dynamic-update-slice_fusion.14
  260.2 1.8 constant_dynamic-update-slice_fusion.13
  262.0 1.9 constant_dynamic-update-slice_fusion.12
  263.9 0.9 constant_dynamic-update-slice_fusion.11
  264.7 0.8 constant_dynamic-update-slice_fusion.10
  265.5 0.8 constant_dynamic-update-slice_fusion.9
  266.3 0.8 constant_dynamic-update-slice_fusion.8
  267.1 1.8 constant_dynamic-update-slice_fusion.7
  268.9 1.8 constant_dynamic-update-slice_fusion.6
  270.7 1.8 constant_dynamic-update-slice_fusion.5
  272.5 0.8 constant_dynamic-update-slice_fusion.4
  273.3 0.8 constant_dynamic-update-slice_fusion.3
  274.2 0.8 constant_dynamic-update-slice_fusion.2
  275.0 0.8 constant_dynamic-update-slice_fusion.1
  275.8 0.8 constant_dynamic-update-slice_fusion
  276.6 8.3 %fusion.31 = f32[1024,1408]{1,0:T(8,128)} fusion(bf16[1024,1024]{1,0:T(8,128)(2,1)} %all-gather.10.cloned.1.call-done, bf16[1024,1408]{1,0:T(8,128)(2,1)} %all-gather.12.cloned.1.call-done), kind=kOutput, calls=%fused_computation.76 | convolution fusion | flops 2952790016 | bytes 10747904 | tf_op jit(solution)/shard_map/dot_general | solution.py:62
  284.9 18.4 %all-gather.14.cloned.1.call-done = bf16[1024,1408]{1,0:T(8,128)(2,1)} async-done(((bf16[128,1408]{1,0:T(8,128)(2,1)}), bf16[1024,1408]{1,0:T(8,128)(2,1)}) %all-gather.14.cloned.1.call-update) | async-done | bytes 2883600 | tf_op jit(solution)/shard_map/all_gather | solution.py:114
  303.4 13.0 %fusion.9 = bf16[1024,1024]{1,0:T(8,128)(2,1)} fusion(bf16[1408,2048]{1,0:T(8,128)(2,1)} %constant_dynamic-update-slice_fusion, s32[]{:T(128)S(6)} %select_n.28, f32[1024,1408]{1,0:T(8,128)} %fusion.31, bf16[1024,1024]{1,0:T(8,128)(2,1)} %all-gather.10.cloned.1.call-done, bf16[1024,1408]{1,0:T(8,128)(2,1)} %all-gather.14.cloned.1.call-done), kind=kOutput, calls=%fused_computation.19 | convolution fusion | flops 5915279360 | bytes 15728644 | tf_op jit(solution)/shard_map/dot_general | solution.py:62
  316.4 8.5 %reduce-scatter.2.cloned.1.call-done = bf16[512,1024]{1,0:T(8,128)(2,1)} async-done(((bf16[1024,1024]{1,0:T(8,128)(2,1)}), bf16[512,1024]{1,0:T(8,128)(2,1)}) %reduce-scatter.2.cloned.1.call-update) | async-done | bytes 1048592 | tf_op jit(solution)/shard_map/reduce_scatter | solution.py:126
  324.9 2.5 add_convert_fusion
  (108 shorter events, 7.8 us)
Async XLA Ops:
  6.5 6.4 %copy-start = (bf16[1024,16]{0,1:T(8,128)(2,1)S(1)}, bf16[1024,16]{0,1:T(8,128)(2,1)}, u32[]{:S(2)}) copy-start(bf16[1024,16]{0,1:T(8,128)(2,1)} %param.21) | copy-start | bytes 98308
  6.5 4.2 %copy-start.11 = (bf16[256,128]{1,0:T(8,128)(2,1)S(1)}, bf16[256,128]{1,0:T(8,128)(2,1)}, u32[]{:S(2)}) copy-start(bf16[256,128]{1,0:T(8,128)(2,1)} %param.25) | copy-start | bytes 196612
  6.5 106.3 %all-gather.6.cloned.1.call-start = ((), (), s32[]{:S(2)}) async-start(), calls=%async_computation.2 | async-start | bytes 3145728 | tf_op jit(solution)/shard_map/all_gather | solution.py:85
  6.5 10.1 %copy-start.17 = (bf16[16,128]{1,0:T(8,128)(2,1)S(1)}, bf16[16,128]{1,0:T(8,128)(2,1)}, u32[]{:S(2)}) copy-start(bf16[16,128]{1,0:T(8,128)(2,1)} %param.22) | copy-start | bytes 12292
  6.5 10.1 %copy-start.18 = (f32[128]{0:T(128)S(1)}, f32[128]{0:T(128)}, u32[]{:S(2)}) copy-start(f32[128]{0:T(128)} %param.23) | copy-start | bytes 1540
  10.6 6.8 %copy-start.12 = (bf16[128,256]{1,0:T(8,128)(2,1)S(1)}, bf16[128,256]{1,0:T(8,128)(2,1)}, u32[]{:S(2)}) copy-start(bf16[128,256]{1,0:T(8,128)(2,1)} %param.20) | copy-start | bytes 196612
  10.6 40.1 %copy-start.13 = (bf16[128,128]{1,0:T(8,128)(2,1)S(1)}, bf16[128,128]{1,0:T(8,128)(2,1)}, u32[]{:S(2)}) copy-start(bf16[128,128]{1,0:T(8,128)(2,1)} %param.18) | copy-start | bytes 98308
  10.7 71.4 %copy-start.14 = (bf16[128,128]{1,0:T(8,128)(2,1)S(1)}, bf16[128,128]{1,0:T(8,128)(2,1)}, u32[]{:S(2)}) copy-start(bf16[128,128]{1,0:T(8,128)(2,1)} %param.19) | copy-start | bytes 98308
  10.7 132.6 %all-gather.8.cloned.1.call-start = ((), (), s32[]{:S(2)}) async-start(), calls=%async_computation.3 | async-start | bytes 1179648 | tf_op jit(solution)/shard_map/all_gather | solution.py:108
  112.8 2.5 copy-start.2
  118.4 1.1 copy-start.4
  132.1 5.3 %copy-start.5 = (bf16[1024,256]{1,0:T(8,128)(2,1)S(1)}, bf16[1024,256]{1,0:T(8,128)(2,1)}, u32[]{:S(2)}) copy-start(bf16[1024,256]{1,0:T(8,128)(2,1)} %copy-done.4) | copy-start | bytes 1572868
  137.4 1.2 copy-start.16
  138.2 7.5 %copy-start.1 = (bf16[512,1024]{1,0:T(8,128)(2,1)S(1)}, bf16[512,1024]{1,0:T(8,128)(2,1)}, u32[]{:S(2)}) copy-start(bf16[512,1024]{1,0:T(8,128)(2,1)} %param.16) | copy-start | bytes 3145732
  139.5 8.4 %copy-start.15 = (f32[1024]{0:T(1024)S(1)}, f32[1024]{0:T(1024)}, u32[]{:S(2)}) copy-start(f32[1024]{0:T(1024)} %param.26) | copy-start | bytes 12292
  139.5 5.4 %all-to-all-start = ((bf16[2,512,256]{1,2,0:T(8,128)(2,1)}), bf16[2,512,256]{1,2,0:T(8,128)(2,1)S(1)}, u32[]{:S(2)}, u32[]{:S(2)}) async-start(bf16[2,512,256]{1,2,0:T(8,128)(2,1)} %multiply_convert_fusion.2), calls=%async_computation | async-start | bytes 1048576 | tf_op jit(solution)/shard_map/all_to_all | solution.py:106
  143.2 133.4 %all-gather.10.cloned.1.call-start = ((), (), s32[]{:S(2)}) async-start(), calls=%async_computation.4 | async-start | bytes 3145728 | tf_op jit(solution)/shard_map/all_gather | solution.py:111
  144.9 0.8 copy-start.3
  147.9 1.9 copy-start.6
  149.2 127.4 %all-gather.12.cloned.1.call-start = ((), (), s32[]{:S(2)}) async-start(), calls=%async_computation.5 | async-start | bytes 3244032 | tf_op jit(solution)/shard_map/all_gather | solution.py:113
  149.7 153.6 %all-gather.14.cloned.1.call-start = ((), (), s32[]{:S(2)}) async-start(), calls=%async_computation.6 | async-start | bytes 3244032 | tf_op jit(solution)/shard_map/all_gather | solution.py:114
  149.8 13.2 %collective-permute-start = (bf16[1408,128]{1,0:T(8,128)(2,1)S(1)}, bf16[1408,128]{1,0:T(8,128)(2,1)S(1)}, u32[]{:S(2)}, u32[]{:S(2)}) collective-permute-start(bf16[1408,128]{1,0:T(8,128)(2,1)S(1)} %copy-done.6), channel_id=1, source_target_pairs={{0,2},{2,4},{4,6},{6,8},{8,10},{10,12},{12,14},{14,0},{1,3},{3,5},... | collective-permute-start | bytes 1081352 | tf_op jit(solution)/shard_map/ppermute | solution.py:119
  163.0 12.3 %collective-permute-start.1 = (bf16[1408,128]{1,0:T(8,128)(2,1)S(1)}, bf16[1408,128]{1,0:T(8,128)(2,1)S(1)}, u32[]{:S(2)}, u32[]{:S(2)}) collective-permute-start(bf16[1408,128]{1,0:T(8,128)(2,1)S(1)} %collective-permute-done), channel_id=1, source_target_pairs={{0,2},{2,4},{4,6},{6,8},{8,10},{10,12},{12,14},{14,0},{1,3},{3,5},... | collective-permute-start | bytes 1081352 | tf_op jit(solution)/shard_map/ppermute | solution.py:119
  175.3 20.8 %collective-permute-start.2 = (bf16[1408,128]{1,0:T(8,128)(2,1)S(1)}, bf16[1408,128]{1,0:T(8,128)(2,1)S(1)}, u32[]{:S(2)}, u32[]{:S(2)}) collective-permute-start(bf16[1408,128]{1,0:T(8,128)(2,1)S(1)} %collective-permute-done.1), channel_id=1, source_target_pairs={{0,2},{2,4},{4,6},{6,8},{8,10},{10,12},{12,14},{14,0},{1,3},{3,5},... | collective-permute-start | bytes 1081352 | tf_op jit(solution)/shard_map/ppermute | solution.py:119
  196.2 0.8 copy-start.7
  196.9 16.4 %collective-permute-start.3 = (bf16[1408,128]{1,0:T(8,128)(2,1)S(1)}, bf16[1408,128]{1,0:T(8,128)(2,1)S(1)}, u32[]{:S(2)}, u32[]{:S(2)}) collective-permute-start(bf16[1408,128]{1,0:T(8,128)(2,1)S(1)} %collective-permute-done.2), channel_id=1, source_target_pairs={{0,2},{2,4},{4,6},{6,8},{8,10},{10,12},{12,14},{14,0},{1,3},{3,5},... | collective-permute-start | bytes 1081352 | tf_op jit(solution)/shard_map/ppermute | solution.py:119
  213.3 0.7 copy-start.9
  214.1 19.5 %collective-permute-start.4 = (bf16[1408,128]{1,0:T(8,128)(2,1)S(1)}, bf16[1408,128]{1,0:T(8,128)(2,1)}, u32[]{:S(2)}, u32[]{:S(2)}) collective-permute-start(bf16[1408,128]{1,0:T(8,128)(2,1)S(1)} %collective-permute-done.3), channel_id=1, source_target_pairs={{0,2},{2,4},{4,6},{6,8},{8,10},{10,12},{12,14},{14,0},{1,3},{3,5},... | collective-permute-start | bytes 1081352 | tf_op jit(solution)/shard_map/ppermute | solution.py:119
  233.6 12.6 %collective-permute-start.5 = (bf16[1408,128]{1,0:T(8,128)(2,1)}, bf16[1408,128]{1,0:T(8,128)(2,1)}, u32[]{:S(2)}, u32[]{:S(2)}) collective-permute-start(bf16[1408,128]{1,0:T(8,128)(2,1)} %collective-permute-done.4), channel_id=1, source_target_pairs={{0,2},{2,4},{4,6},{6,8},{8,10},{10,12},{12,14},{14,0},{1,3},{3,5},... | collective-permute-start | bytes 1081352 | tf_op jit(solution)/shard_map/ppermute | solution.py:119
  233.6 91.3 %reduce-scatter.2.cloned.1.call-start = ((), (), s32[]{:S(2)}) async-start(), calls=%async_computation.7 | async-start | bytes 3145728 | tf_op jit(solution)/shard_map/reduce_scatter | solution.py:126
  246.2 10.4 %collective-permute-start.6 = (bf16[1408,128]{1,0:T(8,128)(2,1)}, bf16[1408,128]{1,0:T(8,128)(2,1)}, u32[]{:S(2)}, u32[]{:S(2)}) collective-permute-start(bf16[1408,128]{1,0:T(8,128)(2,1)} %collective-permute-done.5), channel_id=1, source_target_pairs={{0,2},{2,4},{4,6},{6,8},{8,10},{10,12},{12,14},{14,0},{1,3},{3,5},... | collective-permute-start | bytes 1081352 | tf_op jit(solution)/shard_map/ppermute | solution.py:119
  246.2 17.7 %copy-start.8 = (bf16[1408,128]{1,0:T(8,128)(2,1)S(1)}, bf16[1408,128]{1,0:T(8,128)(2,1)}, u32[]{:S(2)}) copy-start(bf16[1408,128]{1,0:T(8,128)(2,1)} %copy-done.7) | copy-start | bytes 1081348
  262.0 10.5 %copy-start.10 = (bf16[1408,128]{1,0:T(8,128)(2,1)S(1)}, bf16[1408,128]{1,0:T(8,128)(2,1)}, u32[]{:S(2)}) copy-start(bf16[1408,128]{1,0:T(8,128)(2,1)} %copy-done.9) | copy-start | bytes 1081348
Sparse Core Ops, SparseCore 0:
  10.8 13.2 all-gather.5
  26.1 42.6 all-gather.7
  149.3 11.5 all-gather.9
  162.9 75.5 all-gather.11
  240.5 62.8 all-gather.13
  316.5 8.3 reduce-scatter.1
